TPU v7x, 256 devices: a whole 4x4x8 slice. The times are simulated.
256 devices in a mesh: fs: 32 (over z, y), tp: 8 (over x, core).
Axes of the slice: x: 4, y: 4, z: 8, core: 2. Of those that a mesh axis runs over, the one named last changes fastest.
Arguments:
- inputs: bfloat16 [65536, 2048], P('fs'), may hold values from -6 to 6
- cotangents: bfloat16 [3, 65536, 1024], P(None, 'fs', 'tp'), as said below
- factor: bfloat16 [2048, 256], P('fs'), as said below
- weights: float32 [3, 2048, 1024], P(None, 'fs', 'tp'), may hold values from -0.125 to 0.125
- first_moment: float32 [3, 256, 1024], P(None, 'fs', 'tp'), may hold values from -0.6 to 0.6
- second_moment: float32 [3, 256, 1024], P(None, 'fs', 'tp'), may hold values from 0.001 to 0.01
Outputs:
- update: float32 [3, 2048, 1024], P(None, 'fs', 'tp')
- new_weights: float32 [3, 2048, 1024], P(None, 'fs', 'tp')
- copies: bfloat16 [3, 2048, 1024], P(None, None, 'tp')
- new_first: float32 [3, 256, 1024], P(None, 'fs', 'tp')
- new_second: float32 [3, 256, 1024], P(None, 'fs', 'tp')
Inputs may be any that keep to these rules, and one draw needn't show every extreme that they name: A real-valued factor of full rank. real-valued cotangents.
All inputs are finite; a program needn't handle non-finite values.
Results may differ from a plain program's by a relative error of at most 0.0085.
Values may be sent and summed in bfloat16 or wider, within the bound.
No kernel may reach another device: no remote copies, remote signals or barrier semaphores. Data moves between devices by JAX's collectives and lax.ppermute only.
A program may use at most 64 MiB of HBM per device.

v0:
```python
import jax
import jax.numpy as jnp
from jax import lax
from jax.sharding import Mesh
from jax.sharding import PartitionSpec as P

MW = 1024
RANK = 256
FS = ("fs_0", "fs_1")
FS_TP = ("fs_0", "fs_1", "tp_0", "tp_1")
TP = ("tp_0", "tp_1")


def joined_along(blocks, dim):
    blocks = jnp.moveaxis(blocks, 0, dim)
    shape = blocks.shape
    return blocks.reshape(*shape[:dim], shape[dim] * shape[dim + 1], *shape[dim + 2 :])


def sent_to_all(array, axis):
    copies = jnp.broadcast_to(array, (lax.axis_size(axis), *array.shape))
    return lax.all_to_all(copies, axis, split_axis=0, concat_axis=0, tiled=True)


def collect(array, axis, dim):
    return joined_along(sent_to_all(array, axis), dim)


def split_up(array, dim, count):
    before, after = (array.shape[:dim], array.shape[dim + 1 :])
    return jnp.moveaxis(array.reshape(*before, count, -1, *after), dim, 0)


def sent_and_summed(array, axis, dim):
    blocks = split_up(array, dim, lax.axis_size(axis))
    arrived = lax.all_to_all(blocks, axis, split_axis=0, concat_axis=0, tiled=True)
    return arrived.sum(axis=0)


def over_axes(array, axes):
    for axis in axes:
        array = lax.psum(array, axis)
    return array


def on_device(inputs, cotangents, factor, weights, first_moment, second_moment):
    factor_wide = factor.astype(jnp.float32)
    local_gradient = jnp.einsum(
        "td,mtc->dmc", inputs, cotangents, preferred_element_type=jnp.float32
    )
    gradient_high = local_gradient.astype(jnp.bfloat16)
    gradient_low = (local_gradient - gradient_high.astype(jnp.float32)).astype(jnp.bfloat16)
    factor_piece = collect(factor, FS, 0)
    high_term = jnp.einsum(
        "dr,dmc->rmc", factor_piece, gradient_high, preferred_element_type=jnp.float32
    )
    low_term = jnp.einsum(
        "dr,dmc->rmc", factor_piece, gradient_low, preferred_element_type=jnp.float32
    )
    partial_value = high_term + low_term
    summed = sent_and_summed(partial_value, FS, 0)
    projected = jnp.transpose(summed, (1, 0, 2))
    square_sum = over_axes(jnp.sum(projected * projected), FS_TP)
    root_mean = jnp.sqrt(square_sum / (3 * RANK * MW) + 1e-06)
    clip_factor = jnp.minimum(1.0, 0.25 / root_mean)
    clipped = clip_factor * projected
    new_first = 0.9 * first_moment + 0.1 * clipped
    new_second = 0.95 * second_moment + 0.05 * clipped * clipped
    normed = new_first / (jnp.sqrt(new_second) + 1e-08)
    normed_whole = collect(normed, FS, 1)
    update = jnp.einsum("dr,mrc->mdc", factor_wide, normed_whole)
    new_weights = weights - 0.02 * update
    copies = collect(new_weights.astype(jnp.bfloat16), FS, 1)
    return (update, new_weights, copies, new_first, new_second)


def solution(mesh):
    torus = Mesh(mesh.devices.reshape(8, 4, 4, 2), ("fs_0", "fs_1", "tp_0", "tp_1"))
    return jax.shard_map(
        on_device,
        mesh=torus,
        in_specs=(
            P(FS, None),
            P(None, FS, TP),
            P(FS, None),
            P(None, FS, TP),
            P(None, FS, TP),
            P(None, FS, TP),
        ),
        out_specs=(
            P(None, FS, TP),
            P(None, FS, TP),
            P(None, None, TP),
            P(None, FS, TP),
            P(None, FS, TP),
        ),
        check_vma=False,
    )
```

profile of v0, /device:TPU:32, one launch (start us, length us, event | category | flops | bytes accessed | tf_op | source)
XLA Modules:
  0.0 169.0 jit_solution(2127882930247664799)
XLA Ops:
  0.6 0.0 copy-start
  0.6 2.0 %broadcast_in_dim.9 = bf16[32,64,256]{2,1,0:T(8,128)(2,1)} broadcast(bf16[64,256]{1,0:T(8,128)(2,1)} %param.8), dimensions={1,2} | broadcast | bytes 1081344 | tf_op jit(solution)/shard_map/broadcast_in_dim | solution.py:21
  2.6 11.4 %all-to-all-start = ((bf16[32,64,256]{2,1,0:T(8,128)(2,1)}), bf16[32,64,256]{2,1,0:T(8,128)(2,1)S(1)}, u32[]{:S(2)}, u32[]{:S(2)}) async-start(bf16[32,64,256]{2,1,0:T(8,128)(2,1)} %broadcast_in_dim.9), calls=%async_computation | async-start | bytes 2097152 | tf_op jit(solution)/shard_map/all_to_all | solution.py:22
  14.0 0.0 copy-done
  14.0 8.6 %fusion = f32[2048,3,128]{2,0,1:T(8,128)} fusion(bf16[3,2048,128]{2,1,0:T(8,128)(2,1)S(1)} %copy-done, bf16[2048,2048]{1,0:T(8,128)(2,1)} %param.6), kind=kOutput, calls=%fused_computation | convolution fusion | flops 3221225472 | bytes 13107200 | tf_op jit(solution)/shard_map/td,mtc->dmc/dot_general | solution.py:48
  22.6 18.5 %all-to-all-done = bf16[32,64,256]{2,1,0:T(8,128)(2,1)S(1)} async-done(((bf16[32,64,256]{2,1,0:T(8,128)(2,1)}), bf16[32,64,256]{2,1,0:T(8,128)(2,1)S(1)}, u32[]{:S(2)}, u32[]{:S(2)}) %all-to-all-start) | async-done | bytes 1048608 | tf_op jit(solution)/shard_map/all_to_all | solution.py:22
  41.2 0.0 copy-start.1
  41.2 2.7 %fusion.6 = f32[3,128,256]{2,1,0:T(8,128)S(1)} fusion(bf16[2048,256,1]{1,0,2:T(8,128)(2,1)S(1)} %bitcast.38, f32[2048,3,128]{2,0,1:T(8,128)} %fusion), kind=kOutput, calls=%fused_computation.8 | convolution fusion | flops 403439616 | bytes 4587520 | tf_op jit(solution)/shard_map/dr,dmc->rmc/dot_general | solution.py:54
  43.8 0.1 copy-done.1
  44.0 0.0 copy-start.4
  44.0 0.0 copy-start.5
  44.0 0.0 copy-start.2
  44.0 0.0 copy-start.3
  44.0 0.6 fusion.4
  44.7 0.2 copy.27
  44.9 19.9 %all_to_all.20 = f32[32,8,3,128]{3,1,2,0:T(8,128)S(1)} all-to-all(f32[32,8,3,128]{3,1,2,0:T(8,128)S(1)} %copy.28), channel_id=1, replica_groups=mesh['fs_0'=8,'fs_1'=4,'tp_0'=4,'tp_1'=2] {'fs_0','fs_1'}, dimensions={0} | all-to-all | bytes 786432 | tf_op jit(solution)/shard_map/all_to_all | solution.py:36
  64.8 0.6 multiply_reduce_fusion
  65.4 15.6 %psum.28 = f32[]{:T(128)} all-reduce(f32[]{:T(128)} %multiply_reduce_fusion), channel_id=1, replica_groups=mesh['fs_0'=8,'fs_1'=4,'tp_0'=4,'tp_1'=2] {'fs_0'}, use_global_device_ids=true, to_apply=%region_2.0 | all-reduce | flops 1 | bytes 8 | tf_op jit(solution)/shard_map/psum | solution.py:42
  81.0 10.1 %psum.29 = f32[]{:T(128)} all-reduce(f32[]{:T(128)} %psum.28), channel_id=1, replica_groups=mesh['fs_0'=8,'fs_1'=4,'tp_0'=4,'tp_1'=2] {'fs_1'}, use_global_device_ids=true, to_apply=%region_3.0 | all-reduce | flops 1 | bytes 8 | tf_op jit(solution)/shard_map/psum | solution.py:42
  91.0 11.1 %psum.30 = f32[]{:T(128)} all-reduce(f32[]{:T(128)} %psum.29), channel_id=1, replica_groups=mesh['fs_0'=8,'fs_1'=4,'tp_0'=4,'tp_1'=2] {'tp_0'}, use_global_device_ids=true, to_apply=%region_4.0 | all-reduce | flops 1 | bytes 8 | tf_op jit(solution)/shard_map/psum | solution.py:42
  102.1 3.1 %psum.31 = f32[]{:T(128)} all-reduce(f32[]{:T(128)} %psum.30), channel_id=1, replica_groups=mesh['fs_0'=8,'fs_1'=4,'tp_0'=4,'tp_1'=2] {'tp_1'}, use_global_device_ids=true, to_apply=%region_5.0 | all-reduce | flops 1 | bytes 8 | tf_op jit(solution)/shard_map/psum | solution.py:42
  105.9 0.0 copy-done.4
  105.9 0.0 copy-done.5
  105.9 0.6 add_divide_fusion
  106.6 16.5 %all_to_all.21 = bf16[32,3,8,128]{3,2,1,0:T(8,128)(2,1)S(1)} all-to-all(bf16[32,3,8,128]{3,2,1,0:T(8,128)(2,1)S(1)} %broadcast_in_dim.10), channel_id=1, replica_groups=mesh['fs_0'=8,'fs_1'=4,'tp_0'=4,'tp_1'=2] {'fs_0','fs_1'}, dimensions={0} | all-to-all | bytes 393216 | tf_op jit(solution)/shard_map/all_to_all | solution.py:22
  123.1 0.0 copy-done.2
  123.1 0.0 copy-done.3
  123.1 0.8 fusion.13
  123.9 0.4 broadcast_in_dim.11
  124.3 43.4 %all_to_all.22 = bf16[32,3,64,128]{3,2,1,0:T(8,128)(2,1)S(1)} all-to-all(bf16[32,3,64,128]{3,2,1,0:T(8,128)(2,1)S(1)} %broadcast_in_dim.11), channel_id=1, replica_groups=mesh['fs_0'=8,'fs_1'=4,'tp_0'=4,'tp_1'=2] {'fs_0','fs_1'}, dimensions={0} | all-to-all | bytes 3145728 | tf_op jit(solution)/shard_map/all_to_all | solution.py:22
  167.7 1.3 copy.30
  (3 shorter events, 0.1 us)
Async XLA Ops:
  0.6 13.4 %copy-start = (bf16[3,2048,128]{2,1,0:T(8,128)(2,1)S(1)}, bf16[3,2048,128]{2,1,0:T(8,128)(2,1)}, u32[]{:S(2)}) copy-start(bf16[3,2048,128]{2,1,0:T(8,128)(2,1)} %param.7) | copy-start | bytes 4718596
  2.6 38.5 %all-to-all-start = ((bf16[32,64,256]{2,1,0:T(8,128)(2,1)}), bf16[32,64,256]{2,1,0:T(8,128)(2,1)S(1)}, u32[]{:S(2)}, u32[]{:S(2)}) async-start(bf16[32,64,256]{2,1,0:T(8,128)(2,1)} %broadcast_in_dim.9), calls=%async_computation | async-start | bytes 2097152 | tf_op jit(solution)/shard_map/all_to_all | solution.py:22
  41.2 2.8 %copy-start.1 = (f32[2048,3,128]{2,0,1:T(8,128)S(1)}, f32[2048,3,128]{2,0,1:T(8,128)}, u32[]{:S(2)}) copy-start(f32[2048,3,128]{2,0,1:T(8,128)} %fusion) | copy-start | bytes 9437188
  44.0 61.9 %copy-start.4 = (f32[3,8,128]{2,1,0:T(8,128)S(1)}, f32[3,8,128]{2,1,0:T(8,128)}, u32[]{:S(2)}) copy-start(f32[3,8,128]{2,1,0:T(8,128)} %param.11) | copy-start | bytes 36868
  44.0 61.9 %copy-start.5 = (f32[3,8,128]{2,1,0:T(8,128)S(1)}, f32[3,8,128]{2,1,0:T(8,128)}, u32[]{:S(2)}) copy-start(f32[3,8,128]{2,1,0:T(8,128)} %param.10) | copy-start | bytes 36868
  44.0 79.1 %copy-start.2 = (bf16[64,256]{1,0:T(8,128)(2,1)S(1)}, bf16[64,256]{1,0:T(8,128)(2,1)}, u32[]{:S(2)}) copy-start(bf16[64,256]{1,0:T(8,128)(2,1)} %param.8) | copy-start | bytes 98308
  44.0 79.1 %copy-start.3 = (f32[3,64,128]{2,1,0:T(8,128)S(1)}, f32[3,64,128]{2,1,0:T(8,128)}, u32[]{:S(2)}) copy-start(f32[3,64,128]{2,1,0:T(8,128)} %param.9) | copy-start | bytes 294916
where the time goes:
time: 169 us
  blocking collectives  120 us (71%)
  waiting for transfers between devices  18.5 us (11%)
  matrix products  12.8 us (8%)
  starting transfers between devices  11.4 us (7%)
  local copies, waits for them, and re-layouts  4.01 us (2%)
    all_to_all x2, blocking collectives, sent_to_all(): return lax.all_to_all(copies, axis, split_axis=0, concat_axis=0, tiled=True)  59.9 us
    psum x4, blocking collectives, over_axes(): array = lax.psum(array, axis)  39.8 us
    all_to_all x1, blocking collectives, sent_and_summed(): lax.all_to_all(blocks, axis, split_axis=0, concat_axis=0, tiled=True)  19.9 us
    all_to_all x1, waiting for transfers between devices, sent_to_all(): return lax.all_to_all(copies, axis, split_axis=0, concat_axis=0, tiled=True)  18.5 us
    all_to_all x1, starting transfers between devices, sent_to_all(): return lax.all_to_all(copies, axis, split_axis=0, concat_axis=0, tiled=True)  11.4 us
    dot_general x1, matrix products, on_device(): jnp.einsum('td,mtc->dmc', inputs, cotangents, preferred_element_type=jnp....  8.65 us
  transfers between devices with their start and end apart: 1, of which 1 were waited for; matrix products, arithmetic and copies ran while one was open for 5% of the time, Pallas kernels for 0%

commit v1 on v0

--- a/solution.py
+++ b/solution.py
@@ -39,7 +39,8 @@
 
 def over_axes(array, axes):
     for axis in axes:
-        array = lax.psum(array, axis)
+        parts = lax.all_gather(array, axis, axis=0, tiled=False)
+        array = parts.sum(axis=0)
     return array
 
 

time: 169 us -> 178 us (1.053)
  blocking collectives: 120 us -> 97.1 us
  waiting for transfers between devices: 18.5 us -> 31.6 us
  local copies, waits for them, and re-layouts: 4.01 us -> 12.7 us
  starting transfers between devices: 11.4 us -> 17.8 us
  other arithmetic: 1.25 us -> 3.67 us
    psum x4 -> x0, blocking collectives: 39.8 us -> none  [over_axes(): array = lax.psum(array, axis)]
    unnamed x0 -> x4, blocking collectives: none -> 37.3 us
    all_to_all x1 -> x0, blocking collectives: 19.9 us -> none  [sent_and_summed(): lax.all_to_all(blocks, axis, split_axis=0, concat_axis=0, tiled=True)]
    all_to_all x0 -> x1, waiting for transfers between devices: none -> 13.1 us  [sent_and_summed(): lax.all_to_all(blocks, axis, split_axis=0, concat_axis=0, tiled=True)]
    unnamed x12 -> x32, local copies, waits for them, and re-layouts: 0.17 us -> 8.15 us
    all_to_all x0 -> x1, starting transfers between devices: none -> 6.46 us  [sent_and_summed(): lax.all_to_all(blocks, axis, split_axis=0, concat_axis=0, tiled=True)]
    reduce_sum x0 -> x4, other arithmetic: none -> 2.41 us  [over_axes(): array = parts.sum(axis=0)]
  transfers between devices with their start and end apart: 1 -> 2, of which waited for: 1 -> 2; matrix products, arithmetic and copies ran while one was open for 5% -> 5% of each run, Pallas kernels for 0% -> 0%
where the time goes in v1:
time: 178 us; the launch traced here: 177 us
  blocking collectives  97.1 us (55%)
  waiting for transfers between devices  31.6 us (18%)
  starting transfers between devices  17.8 us (10%)
  matrix products  12.8 us (7%)
  local copies, waits for them, and re-layouts  12.7 us (7%)
  other arithmetic  3.67 us (2%)
    all_to_all x2, blocking collectives, sent_to_all(): return lax.all_to_all(copies, axis, split_axis=0, concat_axis=0, tiled=True)  59.9 us
    unnamed x4, blocking collectives  37.3 us
    all_to_all x1, waiting for transfers between devices, sent_to_all(): return lax.all_to_all(copies, axis, split_axis=0, concat_axis=0, tiled=True)  18.5 us
    all_to_all x1, waiting for transfers between devices, sent_and_summed(): lax.all_to_all(blocks, axis, split_axis=0, concat_axis=0, tiled=True)  13.1 us
    all_to_all x1, starting transfers between devices, sent_to_all(): return lax.all_to_all(copies, axis, split_axis=0, concat_axis=0, tiled=True)  11.4 us
    dot_general x1, matrix products, on_device(): jnp.einsum('td,mtc->dmc', inputs, cotangents, preferred_element_type=jnp....  8.65 us
    unnamed x32, local copies, waits for them, and re-layouts  8.15 us
    all_to_all x1, starting transfers between devices, sent_and_summed(): lax.all_to_all(blocks, axis, split_axis=0, concat_axis=0, tiled=True)  6.46 us
  transfers between devices with their start and end apart: 2, of which 2 were waited for; matrix products, arithmetic and copies ran while one was open for 5% of the time, Pallas kernels for 0%

profile of v1, /device:TPU:32, one launch (start us, length us, event | category | flops | bytes accessed | tf_op | source)
XLA Modules:
  0.0 177.2 jit_solution(2339017363665454300)
XLA Ops:
  0.6 2.0 %broadcast_in_dim.9 = bf16[32,64,256]{2,1,0:T(8,128)(2,1)} broadcast(bf16[64,256]{1,0:T(8,128)(2,1)} %param.8), dimensions={1,2} | broadcast | bytes 1081344 | tf_op jit(solution)/shard_map/broadcast_in_dim | solution.py:21
  2.6 11.4 %all-to-all-start = ((bf16[32,64,256]{2,1,0:T(8,128)(2,1)}), bf16[32,64,256]{2,1,0:T(8,128)(2,1)S(1)}, u32[]{:S(2)}, u32[]{:S(2)}) async-start(bf16[32,64,256]{2,1,0:T(8,128)(2,1)} %broadcast_in_dim.9), calls=%async_computation | async-start | bytes 2097152 | tf_op jit(solution)/shard_map/all_to_all | solution.py:22
  14.0 8.6 %fusion = f32[2048,3,128]{2,0,1:T(8,128)} fusion(bf16[3,2048,128]{2,1,0:T(8,128)(2,1)S(1)} %copy-done, bf16[2048,2048]{1,0:T(8,128)(2,1)} %param.6), kind=kOutput, calls=%fused_computation | convolution fusion | flops 3221225472 | bytes 13107200 | tf_op jit(solution)/shard_map/td,mtc->dmc/dot_general | solution.py:49
  22.6 18.5 %all-to-all-done = bf16[32,64,256]{2,1,0:T(8,128)(2,1)S(1)} async-done(((bf16[32,64,256]{2,1,0:T(8,128)(2,1)}), bf16[32,64,256]{2,1,0:T(8,128)(2,1)S(1)}, u32[]{:S(2)}, u32[]{:S(2)}) %all-to-all-start) | async-done | bytes 1048608 | tf_op jit(solution)/shard_map/all_to_all | solution.py:22
  41.2 2.7 %fusion.6 = f32[3,128,256]{2,1,0:T(8,128)S(1)} fusion(bf16[2048,256,1]{1,0,2:T(8,128)(2,1)S(1)} %bitcast.46, f32[2048,3,128]{2,0,1:T(8,128)} %fusion), kind=kOutput, calls=%fused_computation.8 | convolution fusion | flops 403439616 | bytes 4587520 | tf_op jit(solution)/shard_map/dr,dmc->rmc/dot_general | solution.py:55
  44.1 0.6 fusion.4
  44.9 0.8 copy.28
  45.6 6.5 %all-to-all-start.1 = ((f32[32,8,3,128]{3,1,2,0:T(8,128)}), f32[32,8,3,128]{3,1,2,0:T(8,128)S(1)}, u32[]{:S(2)}, u32[]{:S(2)}) async-start(f32[32,8,3,128]{3,1,2,0:T(8,128)} %copy.28), calls=%async_computation.1 | async-start | bytes 786432 | tf_op jit(solution)/shard_map/all_to_all | solution.py:36
  52.1 0.6 dynamic-slice
  52.7 13.1 %all-to-all-done.1 = f32[32,8,3,128]{3,1,2,0:T(8,128)S(1)} async-done(((f32[32,8,3,128]{3,1,2,0:T(8,128)}), f32[32,8,3,128]{3,1,2,0:T(8,128)S(1)}, u32[]{:S(2)}, u32[]{:S(2)}) %all-to-all-start.1) | async-done | bytes 393248 | tf_op jit(solution)/shard_map/all_to_all | solution.py:36
  65.8 0.6 multiply_reduce_fusion
  66.4 1.4 dynamic-update-slice
  67.8 0.6 dynamic-slice.1
  68.4 14.9 %all-reduce = f32[8]{0:T(128)S(1)} all-reduce(f32[8]{0:T(128)S(1)} %dynamic-update-slice), channel_id=1, replica_groups=mesh['fs_0'=8,'fs_1'=4,'tp_0'=4,'tp_1'=2] {'fs_0'}, use_global_device_ids=true, to_apply=%add | all-reduce | flops 8 | bytes 64
  83.3 0.6 reduce_sum.56
  83.9 1.4 dynamic-update-slice.1
  85.3 0.6 dynamic-slice.2
  85.9 9.5 %all-reduce.1 = f32[4]{0:T(128)S(1)} all-reduce(f32[4]{0:T(128)S(1)} %dynamic-update-slice.1), channel_id=1, replica_groups=mesh['fs_0'=8,'fs_1'=4,'tp_0'=4,'tp_1'=2] {'fs_1'}, use_global_device_ids=true, to_apply=%add.1 | all-reduce | flops 4 | bytes 32
  95.4 0.6 reduce_sum.57
  96.0 1.4 dynamic-update-slice.2
  97.4 0.6 dynamic-slice.3
  98.0 10.5 %all-reduce.2 = f32[4]{0:T(128)S(1)} all-reduce(f32[4]{0:T(128)S(1)} %dynamic-update-slice.2), channel_id=1, replica_groups=mesh['fs_0'=8,'fs_1'=4,'tp_0'=4,'tp_1'=2] {'tp_0'}, use_global_device_ids=true, to_apply=%add.2 | all-reduce | flops 4 | bytes 32
  108.4 0.6 reduce_sum.58
  109.0 1.4 dynamic-update-slice.3
  110.4 2.4 %all-reduce.3 = f32[2]{0:T(128)S(1)} all-reduce(f32[2]{0:T(128)S(1)} %dynamic-update-slice.3), channel_id=1, replica_groups=mesh['fs_0'=8,'fs_1'=4,'tp_0'=4,'tp_1'=2] {'tp_1'}, use_global_device_ids=true, to_apply=%add.3 | all-reduce | flops 2 | bytes 16
  112.9 0.6 reduce_sum.59
  114.2 0.6 add_divide_fusion
  114.8 16.5 %all_to_all.20 = bf16[32,3,8,128]{3,2,1,0:T(8,128)(2,1)S(1)} all-to-all(bf16[32,3,8,128]{3,2,1,0:T(8,128)(2,1)S(1)} %broadcast_in_dim.10), channel_id=1, replica_groups=mesh['fs_0'=8,'fs_1'=4,'tp_0'=4,'tp_1'=2] {'fs_0','fs_1'}, dimensions={0} | all-to-all | bytes 393216 | tf_op jit(solution)/shard_map/all_to_all | solution.py:22
  131.3 0.8 fusion.13
  132.2 0.4 broadcast_in_dim.11
  132.5 43.4 %all_to_all.21 = bf16[32,3,64,128]{3,2,1,0:T(8,128)(2,1)S(1)} all-to-all(bf16[32,3,64,128]{3,2,1,0:T(8,128)(2,1)S(1)} %broadcast_in_dim.11), channel_id=1, replica_groups=mesh['fs_0'=8,'fs_1'=4,'tp_0'=4,'tp_1'=2] {'fs_0','fs_1'}, dimensions={0} | all-to-all | bytes 3145728 | tf_op jit(solution)/shard_map/all_to_all | solution.py:22
  175.9 1.3 copy.30
  (27 shorter events, 0.4 us)
Async XLA Ops:
  0.6 13.4 %copy-start = (bf16[3,2048,128]{2,1,0:T(8,128)(2,1)S(1)}, bf16[3,2048,128]{2,1,0:T(8,128)(2,1)}, u32[]{:S(2)}) copy-start(bf16[3,2048,128]{2,1,0:T(8,128)(2,1)} %param.7) | copy-start | bytes 4718596
  2.6 38.5 %all-to-all-start = ((bf16[32,64,256]{2,1,0:T(8,128)(2,1)}), bf16[32,64,256]{2,1,0:T(8,128)(2,1)S(1)}, u32[]{:S(2)}, u32[]{:S(2)}) async-start(bf16[32,64,256]{2,1,0:T(8,128)(2,1)} %broadcast_in_dim.9), calls=%async_computation | async-start | bytes 2097152 | tf_op jit(solution)/shard_map/all_to_all | solution.py:22
  41.2 2.8 %copy-start.1 = (f32[2048,3,128]{2,0,1:T(8,128)S(1)}, f32[2048,3,128]{2,0,1:T(8,128)}, u32[]{:S(2)}) copy-start(f32[2048,3,128]{2,0,1:T(8,128)} %fusion) | copy-start | bytes 9437188
  44.0 8.1 %copy-start.9 = (u32[256]{0:T(256)S(1)}, u32[256]{0:T(256)}, u32[]{:S(2)}) copy-start(u32[256]{0:T(256)} %constant.27) | copy-start | bytes 3076
  44.0 23.8 %copy-start.8 = (u32[256]{0:T(256)S(1)}, u32[256]{0:T(256)}, u32[]{:S(2)}) copy-start(u32[256]{0:T(256)} %constant.32) | copy-start | bytes 3076
  44.0 41.3 %copy-start.7 = (u32[256]{0:T(256)S(1)}, u32[256]{0:T(256)}, u32[]{:S(2)}) copy-start(u32[256]{0:T(256)} %constant.37) | copy-start | bytes 3076
  44.0 53.4 %copy-start.6 = (u32[256]{0:T(256)S(1)}, u32[256]{0:T(256)}, u32[]{:S(2)}) copy-start(u32[256]{0:T(256)} %constant.42) | copy-start | bytes 3076
  44.0 70.2 %copy-start.4 = (f32[3,8,128]{2,1,0:T(8,128)S(1)}, f32[3,8,128]{2,1,0:T(8,128)}, u32[]{:S(2)}) copy-start(f32[3,8,128]{2,1,0:T(8,128)} %param.11) | copy-start | bytes 36868
  44.0 70.2 %copy-start.5 = (f32[3,8,128]{2,1,0:T(8,128)S(1)}, f32[3,8,128]{2,1,0:T(8,128)}, u32[]{:S(2)}) copy-start(f32[3,8,128]{2,1,0:T(8,128)} %param.10) | copy-start | bytes 36868
  44.0 87.3 %copy-start.2 = (bf16[64,256]{1,0:T(8,128)(2,1)S(1)}, bf16[64,256]{1,0:T(8,128)(2,1)}, u32[]{:S(2)}) copy-start(bf16[64,256]{1,0:T(8,128)(2,1)} %param.8) | copy-start | bytes 98308
  44.0 87.3 %copy-start.3 = (f32[3,64,128]{2,1,0:T(8,128)S(1)}, f32[3,64,128]{2,1,0:T(8,128)}, u32[]{:S(2)}) copy-start(f32[3,64,128]{2,1,0:T(8,128)} %param.9) | copy-start | bytes 294916
  45.6 20.1 %all-to-all-start.1 = ((f32[32,8,3,128]{3,1,2,0:T(8,128)}), f32[32,8,3,128]{3,1,2,0:T(8,128)S(1)}, u32[]{:S(2)}, u32[]{:S(2)}) async-start(f32[32,8,3,128]{3,1,2,0:T(8,128)} %copy.28), calls=%async_computation.1 | async-start | bytes 786432 | tf_op jit(solution)/shard_map/all_to_all | solution.py:36
